TPU v7x, 32 devices: a whole 2x2x4 slice. The times are simulated.
32 devices in a mesh: sp: 8 (over z, x), tp: 4 (over y, core).
Axes of the slice: x: 2, y: 2, z: 4, core: 2. Of those that a mesh axis runs over, the one named last changes fastest.
Arguments:
- target: bfloat16 [1024, 4096], P('sp', 'tp'), may hold values from -300 to 300
- gain: float32 [4096], P('tp'), may hold values from 0.1 to 1.9
- w_query: bfloat16 [4096, 4096], P('tp'), may hold values from -0.09375 to 0.09375
- queries: bfloat16 [1024, 4096], P('sp', 'tp'), may hold values from -13 to 13
- keys: bfloat16 [4096, 1024], P('sp'), may hold values from -4 to 4
- values: bfloat16 [4096, 1024], P('sp'), may hold values from -4 to 4
- attn_out: bfloat16 [1024, 4096], P('sp', 'tp'), may hold values from -4 to 4
- grad_out: bfloat16 [1024, 4096], P('sp', 'tp'), may hold values from -64 to 64
Outputs:
- grad_rows: bfloat16 [1024, 4096], P('sp', 'tp')
- grad_weight: float32 [4096, 4096], P(('tp', 'sp'))
- grad_keys: float32 [4096, 1024], P(('sp', 'tp'))
- grad_values: float32 [4096, 1024], P(('sp', 'tp'))
All inputs are finite; a program needn't handle non-finite values.
Results may differ from a plain program's by a relative error of at most 0.018.
Values may be sent and summed in bfloat16 or wider, within the bound.
A program may use at most 64 MiB of HBM per device.

v0:
```python
import math
import jax
import jax.numpy as jnp
from jax import lax
from jax.sharding import PartitionSpec as P

WIDTH = 4096
HEADS = 16
KV_HEADS = 4
HEAD_DIM = 256
norm_eps = 1e-06


def merged(part, axis, combine):
    gathered = jax.tree.map(lambda a: lax.all_gather(a, axis), part)

    def take(source):
        return jax.tree.map(lambda a: lax.dynamic_index_in_dim(a, source, 0, False), gathered)

    return lax.fori_loop(
        1, lax.axis_size(axis), lambda source, state: combine(state, take(source)), take(0)
    )


def join_stats(first_part, second_part):
    row_peak = jnp.maximum(first_part[0], second_part[0])
    summed = first_part[1] * jnp.exp(first_part[0] - row_peak) + second_part[1] * jnp.exp(
        second_part[0] - row_peak
    )
    return (row_peak, summed, first_part[2] + second_part[2])


def local(target, gain, w_query, queries, keys, values, attn_out, grad_out):
    local_heads = queries.shape[1] // HEAD_DIM
    group_size = HEADS // KV_HEADS
    score_scale = HEAD_DIM ** (-0.5)
    own_rows = queries.shape[0]
    src_rows = keys.shape[0]
    kv_index = lax.axis_index("tp") * local_heads // group_size
    key_own = lax.dynamic_slice_in_dim(keys, kv_index * HEAD_DIM, HEAD_DIM, 1)
    value_own = lax.dynamic_slice_in_dim(values, kv_index * HEAD_DIM, HEAD_DIM, 1)
    out_heads = attn_out.reshape(own_rows, local_heads, HEAD_DIM).astype(jnp.float32)
    grad_heads = grad_out.reshape(own_rows, local_heads, HEAD_DIM).astype(jnp.float32)
    delta_own = jnp.sum(out_heads * grad_heads, axis=2)
    empty_sum = jnp.zeros((src_rows, HEAD_DIM), jnp.float32)
    total_rows = own_rows * lax.axis_size("sp")
    position = lax.axis_index("sp") * own_rows
    delta_full = lax.dynamic_update_slice_in_dim(
        jnp.zeros((total_rows, local_heads), jnp.float32), delta_own, position, 0
    )
    query_all, grad_all = (
        lax.all_gather(queries, "sp", axis=0, tiled=True),
        lax.all_gather(grad_out, "sp", axis=0, tiled=True),
    )
    block_rows = math.gcd(total_rows, 512)
    block_count = total_rows // block_rows
    query_blocks = query_all.reshape(block_count, block_rows, local_heads, HEAD_DIM)
    grad_blocks = grad_all.reshape(block_count, block_rows, local_heads, HEAD_DIM)

    def block_stats(query_block):
        scores = (
            jnp.einsum("qhd,sd->hqs", query_block, key_own, preferred_element_type=jnp.float32)
            * score_scale
        )
        row_peak = jnp.max(scores, axis=2)
        row_total = jnp.sum(jnp.exp(scores - row_peak[:, :, None]), axis=2)
        return (row_peak, row_total)

    peaks, totals = lax.map(block_stats, query_blocks)
    peaks, totals, delta_full = merged((peaks, totals, delta_full), "sp", join_stats)
    log_totals = peaks + jnp.log(totals)
    delta_blocks = delta_full.reshape(block_count, block_rows, local_heads)

    def block_grads(running, inputs):
        query_block, grad_block, delta_block, log_block = inputs
        scores = (
            jnp.einsum("qhd,sd->hqs", query_block, key_own, preferred_element_type=jnp.float32)
            * score_scale
        )
        weights = jnp.exp(scores - log_block[:, :, None])
        grad_weights = jnp.einsum(
            "qhd,sd->hqs", grad_block, value_own, preferred_element_type=jnp.float32
        )
        delta_cols = jnp.transpose(delta_block)
        grad_scores = (weights * (grad_weights - delta_cols[:, :, None]) * score_scale).astype(
            jnp.bfloat16
        )
        key_sum = running[0] + jnp.einsum(
            "hqs,qhd->sd", grad_scores, query_block, preferred_element_type=jnp.float32
        )
        value_sum = running[1] + jnp.einsum(
            "hqs,qhd->sd",
            weights.astype(jnp.bfloat16),
            grad_block,
            preferred_element_type=jnp.float32,
        )
        query_part = jnp.einsum(
            "hqs,sd->qhd", grad_scores, key_own, preferred_element_type=jnp.float32
        )
        return ((key_sum, value_sum), query_part)

    (key_sum, value_sum), query_parts = lax.scan(
        block_grads, (empty_sum, empty_sum), (query_blocks, grad_blocks, delta_blocks, log_totals)
    )
    query_parts = query_parts.reshape(total_rows, 1, local_heads * HEAD_DIM)
    received = lax.all_to_all(
        query_parts.astype(jnp.bfloat16), "sp", split_axis=0, concat_axis=1, tiled=True
    ).astype(query_parts.dtype)
    query_grad = jnp.sum(received, axis=1)
    key_cols = key_sum.reshape(src_rows, 1, HEAD_DIM)
    value_cols = value_sum.reshape(src_rows, 1, HEAD_DIM)
    key_parts, value_parts = (
        lax.all_to_all(
            key_cols.astype(jnp.bfloat16), "tp", split_axis=0, concat_axis=1, tiled=True
        ).astype(key_cols.dtype),
        lax.all_to_all(
            value_cols.astype(jnp.bfloat16), "tp", split_axis=0, concat_axis=1, tiled=True
        ).astype(value_cols.dtype),
    )
    part_rows = key_parts.shape[0]
    per_kv = key_parts.shape[1] // KV_HEADS
    grad_keys = (
        key_parts.reshape(part_rows, KV_HEADS, per_kv, HEAD_DIM)
        .sum(axis=2)
        .reshape(part_rows, KV_HEADS * HEAD_DIM)
    )
    grad_values = (
        value_parts.reshape(part_rows, KV_HEADS, per_kv, HEAD_DIM)
        .sum(axis=2)
        .reshape(part_rows, KV_HEADS * HEAD_DIM)
    )
    query_grad = query_grad.astype(jnp.bfloat16)
    query_all_heads = lax.all_gather(query_grad, "tp", axis=1, tiled=True)
    grad_rows = lax.dot_general(
        query_all_heads, w_query, (((1,), (1,)), ((), ())), preferred_element_type=jnp.float32
    ).astype(jnp.bfloat16)
    target_wide = target.astype(jnp.float32)
    squares = lax.psum(jnp.sum(target_wide * target_wide, axis=1), "tp")
    inverse = lax.rsqrt(squares / WIDTH + norm_eps)
    normed = (target_wide * inverse[:, None] * gain).astype(jnp.bfloat16)
    grad_weight = lax.psum_scatter(
        lax.dot_general(
            normed, query_all_heads, (((0,), (0,)), ((), ())), preferred_element_type=jnp.float32
        ).astype(jnp.bfloat16),
        "sp",
        scatter_dimension=0,
        tiled=True,
    ).astype(jnp.float32)
    return (grad_rows, grad_weight, grad_keys, grad_values)


def solution(mesh):
    return jax.shard_map(
        local,
        mesh=mesh,
        in_specs=(
            P("sp", "tp"),
            P("tp"),
            P("tp", None),
            P("sp", "tp"),
            P("sp", None),
            P("sp", None),
            P("sp", "tp"),
            P("sp", "tp"),
        ),
        out_specs=(
            P("sp", "tp"),
            P(("tp", "sp"), None),
            P(("sp", "tp"), None),
            P(("sp", "tp"), None),
        ),
        check_vma=False,
    )
```

profile of v0, /device:TPU:0, one launch (start us, length us, event | category | flops | bytes accessed | tf_op | source)
XLA Modules:
  0.0 421.2 jit_solution(14617625495296849069)
XLA Ops:
  10.4 32.5 %all_gather.33 = f32[8,1024,4]{1,2,0:T(4,128)S(1)} all-gather(f32[1,1024,4]{1,2,0:T(4,128)S(1)} %constant_dynamic-update-slice_fusion), channel_id=1, replica_groups=mesh['sp'=8,'tp'=4] {'sp'}, dimensions={0}, use_global_device_ids=true | all-gather | bytes 147456 | tf_op jit(solution)/shard_map/all_gather | solution.py:15
  45.4 17.0 %all-gather.6.cloned.1.call-done = bf16[1024,1024]{1,0:T(8,128)(2,1)} async-done(((bf16[128,1024]{1,0:T(8,128)(2,1)}), bf16[1024,1024]{1,0:T(8,128)(2,1)}) %all-gather.6.cloned.1.call-update) | async-done | bytes 2097168 | tf_op jit(solution)/shard_map/all_gather | solution.py:52
  62.4 4.5 %reshape.71 = bf16[2,512,4,256]{3,2,1,0:T(4,128)(2,1)} reshape(bf16[1024,1024]{1,0:T(8,128)(2,1)} %all-gather.6.cloned.1.call-done) | data formatting | bytes 4194304 | tf_op jit(solution)/shard_map/reshape | solution.py:57
  71.8 31.3 %all-gather.1 = f32[16,4,512]{2,1,0:T(4,128)S(1)} all-gather(f32[2,4,512]{2,1,0:T(4,128)S(1)} %get-tuple-element.265), channel_id=3, replica_groups=mesh['sp'=8,'tp'=4] {'sp'}, dimensions={0}, use_global_device_ids=true | all-gather | bytes 147456 | tf_op jit(solution)/shard_map/all_gather | solution.py:15
  103.1 30.8 %all-gather = f32[16,4,512]{2,1,0:T(4,128)S(1)} all-gather(f32[2,4,512]{2,1,0:T(4,128)S(1)} %get-tuple-element.264), channel_id=2, replica_groups=mesh['sp'=8,'tp'=4] {'sp'}, dimensions={0}, use_global_device_ids=true | all-gather | bytes 147456 | tf_op jit(solution)/shard_map/all_gather | solution.py:15
  134.5 10.6 %while.47 = (s32[]{:T(128)}, f32[2,4,512]{2,1,0:T(4,128)S(1)}, f32[2,4,512]{2,1,0:T(4,128)S(1)}, f32[1024,4]{0,1:T(4,128)S(1)}, f32[8,2,4,512]{3,2,1,0:T(4,128)}...) while((s32[]{:T(128)}, f32[2,4,512]{2,1,0:T(4,128)S(1)}, ...), condition=%wide.region_6.7_spmd, body=%wide.region_5.6_spmd.sunk | while | flops 28677 | bytes 147599 | solution.py:20
  145.2 4.5 %reshape.72 = bf16[2,512,4,256]{3,2,1,0:T(4,128)(2,1)} reshape(bf16[1024,1024]{1,0:T(8,128)(2,1)} %all-gather.8.cloned.1.call-done) | data formatting | bytes 4194304 | tf_op jit(solution)/shard_map/reshape | solution.py:58
  149.6 18.0 %while.48 = (s32[]{:T(128)}, f32[512,256]{1,0:T(8,128)S(1)}, f32[512,256]{1,0:T(8,128)S(1)}, bf16[2,512,4,256]{3,1,2,0:T(8,128)(2,1)}, bf16[2,512,4,256]{3,1,2,0...) while((s32[]{:T(128)}, f32[512,256]{1,0:T(8,128)S(1)}, ...), condition=%wide.region_8.9_spmd.clone, body=%wide.region_7.8_spmd.clone.sunk | while | flops 2694316032 | bytes 48029940 | solution.py:102
  167.7 3.2 copy.40
  170.9 6.3 %convert_element_type.92 = bf16[1024,1,1024]{2,1,0:T(2,128)(2,1)} reshape(bf16[2,512,4,256]{3,2,1,0:T(4,128)(2,1)S(1)} %copy.40) | data formatting | bytes 4194304 | tf_op jit(solution)/shard_map/convert_element_type | solution.py:107
  177.7 12.8 %reduce.4 = bf16[1024,1024]{1,0:T(8,128)(2,1)S(1)} reduce(bf16[1024,1,1024]{2,1,0:T(2,128)(2,1)} %convert_element_type.92, bf16[]{:T(256)} %broadcast.49), dimensions={1}, to_apply=%convert_element_type.92.reduce_sub_computation | reduce | bytes 4194306 | tf_op jit(solution)/shard_map/convert_element_type | solution.py:107
  190.5 3.8 reshape.99
  194.2 38.8 %all_to_all.30 = bf16[8,2,65536]{2,1,0:T(2,128)(2,1)S(1)} all-to-all(bf16[8,2,65536]{2,1,0:T(2,128)(2,1)} %reshape.99), channel_id=1, replica_groups=mesh['sp'=8,'tp'=4] {'sp'}, dimensions={0} | all-to-all | bytes 4194304 | tf_op jit(solution)/shard_map/all_to_all | solution.py:106
  233.0 4.3 %reshape.100 = bf16[1024,1,1024]{2,1,0:T(2,128)(2,1)} reshape(bf16[8,2,65536]{2,1,0:T(2,128)(2,1)S(1)} %all_to_all.30) | data formatting | bytes 4194304
  237.3 3.0 copy.49
  241.7 5.9 %psum.7 = f32[128]{0:T(128)S(1)} all-reduce(f32[128]{0:T(128)S(1)} %fusion.36), channel_id=1, replica_groups=mesh['sp'=8,'tp'=4] {'tp'}, use_global_device_ids=true, to_apply=%region_11.12 | all-reduce | flops 128 | bytes 1024 | tf_op jit(solution)/shard_map/psum | solution.py:138
  247.6 9.8 %all-gather.10.cloned.1.call-done = bf16[128,4096]{1,0:T(8,128)(2,1)} async-done(((bf16[128,1024]{1,0:T(8,128)(2,1)}), bf16[128,4096]{1,0:T(8,128)(2,1)}) %all-gather.10.cloned.1.call-update) | async-done | bytes 1048592 | tf_op jit(solution)/shard_map/all_gather | solution.py:133
  257.4 6.9 %convolution_convert_fusion = bf16[1024,4096]{1,0:T(8,128)(2,1)} fusion(bf16[128,4096]{1,0:T(8,128)(2,1)} %all-gather.10.cloned.1.call-done, bf16[128,1024]{1,0:T(8,128)(2,1)S(1)} %copy-done.3, f32[1024]{0:T(1024)S(1)} %copy-done.8, f32[128]{0:T(128)S(1)} %add_rsqrt_fusion), kind=kOutput, calls=%fused_computation.47 | convolution fusion | flops 1078460416 | bytes 9703936 | tf_op jit(solution)/shard_map/dot_general | solution.py:142
  265.9 3.4 all-to-all-start.1
  270.9 4.3 %all-to-all-done.1 = bf16[4,2,16384]{2,1,0:T(2,128)(2,1)S(1)} async-done(((bf16[4,2,16384]{2,1,0:T(2,128)(2,1)}), bf16[4,2,16384]{2,1,0:T(2,128)(2,1)S(1)}, u32[]{:S(2)}, u32[]{:S(2)}) %all-to-all-start.1) | async-done | bytes 262176 | tf_op jit(solution)/shard_map/all_to_all | solution.py:113
  275.3 3.4 all-to-all-start.2
  280.8 3.9 all-to-all-done.2
  286.7 7.0 %convolution_convert_fusion.1 = bf16[128,1024]{1,0:T(8,128)(2,1)} fusion(bf16[128,4096]{1,0:T(8,128)(2,1)S(1)} %copy-done, bf16[1024,4096]{1,0:T(8,128)(2,1)} %param.16), kind=kOutput, calls=%fused_computation.48 | convolution fusion | flops 1073872896 | bytes 9699328 | tf_op jit(solution)/shard_map/dot_general | solution.py:134
  293.8 118.1 %reduce-scatter.2.cloned.1.call-done = bf16[128,4096]{1,0:T(8,128)(2,1)} async-done(((bf16[1024,4096]{1,0:T(8,128)(2,1)}), bf16[128,4096]{1,0:T(8,128)(2,1)}) %reduce-scatter.2.cloned.1.call-update) | async-done | bytes 1048592 | tf_op jit(solution)/shard_map/reduce_scatter | solution.py:141
  (106 shorter events, 54.3 us)
Async XLA Ops:
  7.2 55.2 %all-gather.6.cloned.1.call-start = ((), (), s32[]{:S(2)}) async-start(), calls=%async_computation.4 | async-start | bytes 2359296 | tf_op jit(solution)/shard_map/all_gather | solution.py:52
  7.9 137.2 %all-gather.8.cloned.1.call-start = ((), (), s32[]{:S(2)}) async-start(), calls=%async_computation.5 | async-start | bytes 2359296 | tf_op jit(solution)/shard_map/all_gather | solution.py:53
  8.6 248.7 %all-gather.10.cloned.1.call-start = ((), (), s32[]{:S(2)}) async-start(), calls=%async_computation.6 | async-start | bytes 1310720 | tf_op jit(solution)/shard_map/all_gather | solution.py:133
  42.9 0.7 copy-start.4
  103.0 30.8 %copy-start.5 = (f32[16,4,512]{2,1,0:T(4,128)}, f32[16,4,512]{2,1,0:T(4,128)S(1)}, u32[]{:S(2)}) copy-start(f32[16,4,512]{2,1,0:T(4,128)S(1)} %all-gather.1) | copy-start | bytes 393220
  133.8 0.7 copy-start.6
  152.0 1.5 copy-start.7
  155.0 1.6 copy-start.1
  157.3 1.3 copy-start.2
  161.0 1.5 copy-start.7
  164.0 1.6 copy-start.1
  166.3 1.3 copy-start.2
  237.3 4.2 %copy-start.3 = (bf16[128,1024]{1,0:T(8,128)(2,1)S(1)}, bf16[128,1024]{1,0:T(8,128)(2,1)}, u32[]{:S(2)}) copy-start(bf16[128,1024]{1,0:T(8,128)(2,1)} %param.14) | copy-start | bytes 786436
  237.3 20.0 %copy-start.8 = (f32[1024]{0:T(1024)S(1)}, f32[1024]{0:T(1024)}, u32[]{:S(2)}) copy-start(f32[1024]{0:T(1024)} %param.15) | copy-start | bytes 12292
  241.5 170.4 %reduce-scatter.2.cloned.1.call-start = ((), (), s32[]{:S(2)}) async-start(), calls=%async_computation.7 | async-start | bytes 9437184 | tf_op jit(solution)/shard_map/reduce_scatter | solution.py:141
  265.9 9.4 %all-to-all-start.1 = ((bf16[4,2,16384]{2,1,0:T(2,128)(2,1)}), bf16[4,2,16384]{2,1,0:T(2,128)(2,1)S(1)}, u32[]{:S(2)}, u32[]{:S(2)}) async-start(bf16[4,2,16384]{2,1,0:T(2,128)(2,1)} %reshape.101), calls=%async_computation.2 | async-start | bytes 524288 | tf_op jit(solution)/shard_map/all_to_all | solution.py:113
  270.9 15.8 %copy-start = (bf16[128,4096]{1,0:T(8,128)(2,1)S(1)}, bf16[128,4096]{1,0:T(8,128)(2,1)}, u32[]{:S(2)}) copy-start(bf16[128,4096]{1,0:T(8,128)(2,1)} %all-gather.10.cloned.1.call-done) | copy-start | bytes 3145732
  275.3 9.4 %all-to-all-start.2 = ((bf16[4,2,16384]{2,1,0:T(2,128)(2,1)}), bf16[4,2,16384]{2,1,0:T(2,128)(2,1)S(1)}, u32[]{:S(2)}, u32[]{:S(2)}) async-start(bf16[4,2,16384]{2,1,0:T(2,128)(2,1)} %reshape.103), calls=%async_computation.3 | async-start | bytes 524288 | tf_op jit(solution)/shard_map/all_to_all | solution.py:116
Sparse Core Ops, SparseCore 0:
  10.1 52.2 all-gather.5
  64.5 49.3 all-gather.7
  241.6 15.6 all-gather.9
  264.4 147.4 reduce-scatter.1
where the time goes:
time: 424 us; the launch traced here: 421 us
  waiting for transfers between devices  155 us (37%)
  blocking collectives  139 us (33%)
  local copies, waits for them, and re-layouts  47.3 us (11%)
  other arithmetic  32.8 us (8%)
  matrix products  26 us (6%)
  between operations  14 us (3%)
  starting transfers between devices  6.97 us (2%)
    reduce_scatter x1, waiting for transfers between devices, local(): lax.psum_scatter(lax.dot_general(normed, query_all_heads, (((0,), (0,)),...  118 us
    all_gather x3, blocking collectives, merged(): gathered = jax.tree.map(lambda a: lax.all_gather(a, axis), part)  94.6 us
    all_to_all x1, blocking collectives, local(): lax.all_to_all(query_parts.astype(jnp.bfloat16), 'sp', split_axis=0, conc...  38.8 us
    unnamed x22, local copies, waits for them, and re-layouts  18.2 us
    all_gather x1, waiting for transfers between devices, local(): lax.all_gather(queries, 'sp', axis=0, tiled=True)  17 us
    convert_element_type x1, other arithmetic, local(): query_parts.astype(jnp.bfloat16)  12.8 us
    convert_element_type x3, local copies, waits for them, and re-layouts, local(): query_parts.astype(jnp.bfloat16)  10 us
    all_gather x1, waiting for transfers between devices, local(): query_all_heads = lax.all_gather(query_grad, 'tp', axis=1, tiled=True)  9.77 us
  transfers between devices with their start and end apart: 6, of which 5 were waited for; matrix products, arithmetic and copies ran while one was open for 9% of the time, Pallas kernels for 0%

commit v1 on v0

--- a/solution.py
+++ b/solution.py
@@ -103,8 +103,14 @@
         block_grads, (empty_sum, empty_sum), (query_blocks, grad_blocks, delta_blocks, log_totals)
     )
     query_parts = query_parts.reshape(total_rows, 1, local_heads * HEAD_DIM)
-    received = lax.all_to_all(
-        query_parts.astype(jnp.bfloat16), "sp", split_axis=0, concat_axis=1, tiled=True
+    received = jnp.concatenate(
+        lax.all_to_all(
+            jnp.stack(jnp.split(query_parts.astype(jnp.bfloat16), lax.axis_size("sp"), axis=0)),
+            "sp",
+            0,
+            0,
+        ),
+        axis=1,
     ).astype(query_parts.dtype)
     query_grad = jnp.sum(received, axis=1)
     key_cols = key_sum.reshape(src_rows, 1, HEAD_DIM)

time: 424 us -> 397 us (0.936)
  other arithmetic: 32.8 us -> 20 us
  local copies, waits for them, and re-layouts: 47.3 us -> 34.6 us
    convert_element_type x1 -> x0, other arithmetic: 12.8 us -> none  [local(): query_parts.astype(jnp.bfloat16)]
    unnamed x22 -> x26, local copies, waits for them, and re-layouts: 18.2 us -> 7.17 us
    convert_element_type x3 -> x2, local copies, waits for them, and re-layouts: 10 us -> 7.78 us  [local(): query_parts.astype(jnp.bfloat16)]
  transfers between devices with their start and end apart: 6 -> 6, of which waited for: 5 -> 5; matrix products, arithmetic and copies ran while one was open for 9% -> 10% of each run, Pallas kernels for 0% -> 0%
where the time goes in v1:
time: 397 us; the launch traced here: 395 us
  waiting for transfers between devices  154 us (39%)
  blocking collectives  139 us (35%)
  local copies, waits for them, and re-layouts  34.6 us (9%)
  matrix products  26.1 us (7%)
  other arithmetic  20 us (5%)
  between operations  14.1 us (4%)
  starting transfers between devices  6.97 us (2%)
    reduce_scatter x1, waiting for transfers between devices, local(): lax.psum_scatter(lax.dot_general(normed, query_all_heads, (((0,), (0,)),...  118 us
    all_gather x3, blocking collectives, merged(): gathered = jax.tree.map(lambda a: lax.all_gather(a, axis), part)  94.4 us
    all_to_all x1, blocking collectives, local(): lax.all_to_all(jnp.stack(jnp.split(query_parts.astype(jnp.bfloat16), lax....  38.5 us
    all_gather x1, waiting for transfers between devices, local(): lax.all_gather(queries, 'sp', axis=0, tiled=True)  17 us
    all_gather x1, waiting for transfers between devices, local(): query_all_heads = lax.all_gather(query_grad, 'tp', axis=1, tiled=True)  9.8 us
  transfers between devices with their start and end apart: 6, of which 5 were waited for; matrix products, arithmetic and copies ran while one was open for 10% of the time, Pallas kernels for 0%

profile of v1, /device:TPU:0, one launch (start us, length us, event | category | flops | bytes accessed | tf_op | source)
XLA Modules:
  0.0 394.8 jit_solution(2137687668849269552)
XLA Ops:
  10.4 32.5 %all_gather.33 = f32[8,1024,4]{1,2,0:T(4,128)S(1)} all-gather(f32[1,1024,4]{1,2,0:T(4,128)S(1)} %constant_dynamic-update-slice_fusion), channel_id=1, replica_groups=mesh['sp'=8,'tp'=4] {'sp'}, dimensions={0}, use_global_device_ids=true | all-gather | bytes 147456 | tf_op jit(solution)/shard_map/all_gather | solution.py:15
  43.6 1.8 constant_dynamic-slice_fusion.1
  45.4 17.0 %all-gather.6.cloned.1.call-done = bf16[1024,1024]{1,0:T(8,128)(2,1)} async-done(((bf16[128,1024]{1,0:T(8,128)(2,1)}), bf16[1024,1024]{1,0:T(8,128)(2,1)}) %all-gather.6.cloned.1.call-update) | async-done | bytes 2097168 | tf_op jit(solution)/shard_map/all_gather | solution.py:52
  62.4 4.5 %reshape.72 = bf16[2,512,4,256]{3,2,1,0:T(4,128)(2,1)} reshape(bf16[1024,1024]{1,0:T(8,128)(2,1)} %all-gather.6.cloned.1.call-done) | data formatting | bytes 4194304 | tf_op jit(solution)/shard_map/reshape | solution.py:57
  66.9 1.9 copy.44
  68.7 3.0 while.46
  71.8 31.3 %all-gather.1 = f32[16,4,512]{2,1,0:T(4,128)S(1)} all-gather(f32[2,4,512]{2,1,0:T(4,128)S(1)} %get-tuple-element.265), channel_id=3, replica_groups=mesh['sp'=8,'tp'=4] {'sp'}, dimensions={0}, use_global_device_ids=true | all-gather | bytes 147456 | tf_op jit(solution)/shard_map/all_gather | solution.py:15
  103.0 30.6 %all-gather = f32[16,4,512]{2,1,0:T(4,128)S(1)} all-gather(f32[2,4,512]{2,1,0:T(4,128)S(1)} %get-tuple-element.264), channel_id=2, replica_groups=mesh['sp'=8,'tp'=4] {'sp'}, dimensions={0}, use_global_device_ids=true | all-gather | bytes 147456 | tf_op jit(solution)/shard_map/all_gather | solution.py:15
  134.3 10.6 %while.47 = (s32[]{:T(128)}, f32[2,4,512]{2,1,0:T(4,128)S(1)}, f32[2,4,512]{2,1,0:T(4,128)S(1)}, f32[1024,4]{0,1:T(4,128)S(1)}, f32[8,2,4,512]{3,2,1,0:T(4,128)}...) while((s32[]{:T(128)}, f32[2,4,512]{2,1,0:T(4,128)S(1)}, ...), condition=%wide.region_6.7_spmd, body=%wide.region_5.6_spmd.sunk | while | flops 28677 | bytes 147599 | solution.py:20
  145.0 4.5 %reshape.73 = bf16[2,512,4,256]{3,2,1,0:T(4,128)(2,1)} reshape(bf16[1024,1024]{1,0:T(8,128)(2,1)} %all-gather.8.cloned.1.call-done) | data formatting | bytes 4194304 | tf_op jit(solution)/shard_map/reshape | solution.py:58
  149.5 18.0 %while.48 = (s32[]{:T(128)}, f32[512,256]{1,0:T(8,128)S(1)}, f32[512,256]{1,0:T(8,128)S(1)}, bf16[2,512,4,256]{3,1,2,0:T(8,128)(2,1)}, bf16[2,512,4,256]{3,1,2,0...) while((s32[]{:T(128)}, f32[512,256]{1,0:T(8,128)S(1)}, ...), condition=%wide.region_8.9_spmd.clone, body=%wide.region_7.8_spmd.clone.sunk | while | flops 2694316032 | bytes 48029940 | solution.py:102
  167.5 4.5 %copy.46 = bf16[2,512,4,256]{3,2,1,0:T(4,128)(2,1)} copy(bf16[2,512,4,256]{3,1,2,0:T(8,128)(2,1)} %get-tuple-element.269) | data formatting | bytes 4194304 | tf_op jit(solution)/shard_map/convert_element_type | solution.py:108
  172.0 3.2 convert_element_type.76
  175.5 38.5 %all_to_all.23 = bf16[8,128,1,1024]{3,1,2,0:T(8,128)(2,1)S(1)} all-to-all(bf16[8,128,1,1024]{3,1,2,0:T(8,128)(2,1)S(1)} %fusion.40), channel_id=1, replica_groups=mesh['sp'=8,'tp'=4] {'sp'}, dimensions={0} | all-to-all | bytes 4194304 | tf_op jit(solution)/shard_map/all_to_all | solution.py:107
  215.3 5.8 %psum.7 = f32[128]{0:T(128)S(1)} all-reduce(f32[128]{0:T(128)S(1)} %fusion.36), channel_id=1, replica_groups=mesh['sp'=8,'tp'=4] {'tp'}, use_global_device_ids=true, to_apply=%region_11.12 | all-reduce | flops 128 | bytes 1024 | tf_op jit(solution)/shard_map/psum | solution.py:144
  221.2 9.8 %all-gather.10.cloned.1.call-done = bf16[128,4096]{1,0:T(8,128)(2,1)} async-done(((bf16[128,1024]{1,0:T(8,128)(2,1)}), bf16[128,4096]{1,0:T(8,128)(2,1)}) %all-gather.10.cloned.1.call-update) | async-done | bytes 1048592 | tf_op jit(solution)/shard_map/all_gather | solution.py:139
  231.0 6.9 %convolution_convert_fusion = bf16[1024,4096]{1,0:T(8,128)(2,1)} fusion(bf16[128,4096]{1,0:T(8,128)(2,1)} %all-gather.10.cloned.1.call-done, bf16[128,1024]{1,0:T(8,128)(2,1)S(1)} %copy-done.3, f32[1024]{0:T(1024)S(1)} %copy-done.8, f32[128]{0:T(128)S(1)} %add_rsqrt_fusion), kind=kOutput, calls=%fused_computation.47 | convolution fusion | flops 1078460416 | bytes 9703936 | tf_op jit(solution)/shard_map/dot_general | solution.py:148
  240.1 3.4 all-to-all-start.1
  245.1 4.4 %all-to-all-done.1 = bf16[4,2,16384]{2,1,0:T(2,128)(2,1)S(1)} async-done(((bf16[4,2,16384]{2,1,0:T(2,128)(2,1)}), bf16[4,2,16384]{2,1,0:T(2,128)(2,1)S(1)}, u32[]{:S(2)}, u32[]{:S(2)}) %all-to-all-start.1) | async-done | bytes 262176 | tf_op jit(solution)/shard_map/all_to_all | solution.py:119
  249.4 3.4 all-to-all-start.2
  254.9 3.9 all-to-all-done.2
  260.9 7.0 %convolution_convert_fusion.1 = bf16[128,1024]{1,0:T(8,128)(2,1)} fusion(bf16[128,4096]{1,0:T(8,128)(2,1)S(1)} %copy-done, bf16[1024,4096]{1,0:T(8,128)(2,1)} %param.16), kind=kOutput, calls=%fused_computation.48 | convolution fusion | flops 1073872896 | bytes 9699328 | tf_op jit(solution)/shard_map/dot_general | solution.py:140
  267.9 117.6 %reduce-scatter.2.cloned.1.call-done = bf16[128,4096]{1,0:T(8,128)(2,1)} async-done(((bf16[1024,4096]{1,0:T(8,128)(2,1)}), bf16[128,4096]{1,0:T(8,128)(2,1)}) %reduce-scatter.2.cloned.1.call-update) | async-done | bytes 1048592 | tf_op jit(solution)/shard_map/reduce_scatter | solution.py:147
  385.6 2.8 convert_element_type.81
  (110 shorter events, 45.1 us)
Async XLA Ops:
  7.2 55.2 %all-gather.6.cloned.1.call-start = ((), (), s32[]{:S(2)}) async-start(), calls=%async_computation.4 | async-start | bytes 2359296 | tf_op jit(solution)/shard_map/all_gather | solution.py:52
  7.9 137.1 %all-gather.8.cloned.1.call-start = ((), (), s32[]{:S(2)}) async-start(), calls=%async_computation.5 | async-start | bytes 2359296 | tf_op jit(solution)/shard_map/all_gather | solution.py:53
  8.6 222.4 %all-gather.10.cloned.1.call-start = ((), (), s32[]{:S(2)}) async-start(), calls=%async_computation.6 | async-start | bytes 1310720 | tf_op jit(solution)/shard_map/all_gather | solution.py:139
  42.9 0.7 copy-start.4
  103.0 30.6 %copy-start.5 = (f32[16,4,512]{2,1,0:T(4,128)}, f32[16,4,512]{2,1,0:T(4,128)S(1)}, u32[]{:S(2)}) copy-start(f32[16,4,512]{2,1,0:T(4,128)S(1)} %all-gather.1) | copy-start | bytes 393220
  133.7 0.7 copy-start.6
  151.8 1.5 copy-start.7
  154.9 1.6 copy-start.1
  157.2 1.3 copy-start.2
  160.8 1.5 copy-start.7
  163.9 1.6 copy-start.1
  166.2 1.3 copy-start.2
  214.0 1.2 copy-start.3
  214.0 17.0 %copy-start.8 = (f32[1024]{0:T(1024)S(1)}, f32[1024]{0:T(1024)}, u32[]{:S(2)}) copy-start(f32[1024]{0:T(1024)} %param.15) | copy-start | bytes 12292
  215.2 170.4 %reduce-scatter.2.cloned.1.call-start = ((), (), s32[]{:S(2)}) async-start(), calls=%async_computation.7 | async-start | bytes 9437184 | tf_op jit(solution)/shard_map/reduce_scatter | solution.py:147
  240.1 9.4 %all-to-all-start.1 = ((bf16[4,2,16384]{2,1,0:T(2,128)(2,1)}), bf16[4,2,16384]{2,1,0:T(2,128)(2,1)S(1)}, u32[]{:S(2)}, u32[]{:S(2)}) async-start(bf16[4,2,16384]{2,1,0:T(2,128)(2,1)} %reshape.100), calls=%async_computation.2 | async-start | bytes 524288 | tf_op jit(solution)/shard_map/all_to_all | solution.py:119
  249.4 9.4 %all-to-all-start.2 = ((bf16[4,2,16384]{2,1,0:T(2,128)(2,1)}), bf16[4,2,16384]{2,1,0:T(2,128)(2,1)S(1)}, u32[]{:S(2)}, u32[]{:S(2)}) async-start(bf16[4,2,16384]{2,1,0:T(2,128)(2,1)} %reshape.102), calls=%async_computation.3 | async-start | bytes 524288 | tf_op jit(solution)/shard_map/all_to_all | solution.py:122
  254.9 6.0 %copy-start = (bf16[128,4096]{1,0:T(8,128)(2,1)S(1)}, bf16[128,4096]{1,0:T(8,128)(2,1)}, u32[]{:S(2)}) copy-start(bf16[128,4096]{1,0:T(8,128)(2,1)} %all-gather.10.cloned.1.call-done) | copy-start | bytes 3145732
Sparse Core Ops, SparseCore 0:
  10.1 52.2 all-gather.5
  64.5 49.3 all-gather.7
  215.3 15.6 all-gather.9
  238.0 147.4 reduce-scatter.1
